TPU v7x, 32 devices: a whole 2x2x4 slice. The times are simulated.
32 devices in a mesh: ra: 8 (over z, x), cb: 4 (over y, core).
Axes of the slice: x: 2, y: 2, z: 4, core: 2. Of those that a mesh axis runs over, the one named last changes fastest.
Arguments:
- tokens: bfloat16 [64, 1024], P(None, 'ra'), may hold values from -14 to 14, as said below
- norm_gain_a: float32 [1024], P('ra'), may hold values from 0.1 to 1.9
- gate_weight_a: float32 [1024, 2816], P('ra', 'cb'), may hold values from -0.1875 to 0.1875
- up_weight_a: float32 [1024, 2816], P('ra', 'cb'), may hold values from -0.1875 to 0.1875
- down_weight_a: float32 [2816, 1024], P('cb', 'ra'), may hold values from -0.109375 to 0.109375
- norm_gain_b: float32 [1024], P('ra'), may hold values from 0.1 to 1.9
- gate_weight_b: float32 [1024, 2816], P('ra', 'cb'), may hold values from -0.1875 to 0.1875
- up_weight_b: float32 [1024, 2816], P('ra', 'cb'), may hold values from -0.1875 to 0.1875
- down_weight_b: float32 [2816, 1024], P('cb', 'ra'), may hold values from -0.109375 to 0.109375
Outputs:
- stream_out: bfloat16 [64, 1024], P(None, 'ra')
Inputs may be any that keep to these rules, and one draw needn't show every extreme that they name: Each feature of tokens carries its own scale, between about 0.3 and 3.3 across features; entries lie within -14 to 14.
All inputs are finite; a program needn't handle non-finite values.
Results may differ from a plain program's by a relative error of at most 0.008.
Values may be sent and summed in bfloat16 or wider, within the bound.
A program may use at most 64 MiB of HBM per device.

v0:
```python
import jax
import jax.numpy as jnp
from jax import lax
from jax.sharding import PartitionSpec as P

residual_weight = 0.5
epsilon = 1e-06


def hidden_of(normed, gate_cast, up_cast):
    gate_part = jnp.dot(normed, gate_cast, preferred_element_type=jnp.float32)
    up_part = jnp.dot(normed, up_cast, preferred_element_type=jnp.float32)
    gate_sum, up_sum = lax.psum((gate_part, up_part), "ra")
    return (jax.nn.silu(gate_sum) * up_sum).astype(jnp.bfloat16)


def normalize(as_float, square_total, gain):
    feature_count = as_float.shape[1] * lax.axis_size("ra")
    row_scale = lax.rsqrt(square_total / feature_count + epsilon)
    return (as_float * row_scale[:, None] * gain).astype(jnp.bfloat16)


def whole_sublayer(stream, gain, gate_weight, up_weight, down_weight):
    as_float = stream.astype(jnp.float32)
    square_total = lax.psum(jnp.sum(as_float * as_float, axis=1), "ra")
    normed = normalize(as_float, square_total, gain)
    hidden = hidden_of(normed, gate_weight.astype(jnp.bfloat16), up_weight.astype(jnp.bfloat16))
    branch_part = jnp.dot(
        hidden, down_weight.astype(jnp.bfloat16), preferred_element_type=jnp.float32
    )
    branch = lax.psum(branch_part, "cb")
    return (residual_weight * as_float + branch).astype(jnp.bfloat16)


def per_device(
    tokens,
    norm_gain_a,
    gate_weight_a,
    up_weight_a,
    down_weight_a,
    norm_gain_b,
    gate_weight_b,
    up_weight_b,
    down_weight_b,
):
    middle = whole_sublayer(tokens, norm_gain_a, gate_weight_a, up_weight_a, down_weight_a)
    return whole_sublayer(middle, norm_gain_b, gate_weight_b, up_weight_b, down_weight_b)


def solution(mesh):
    placed = (
        P(None, "ra"),
        P("ra"),
        P("ra", "cb"),
        P("ra", "cb"),
        P("cb", "ra"),
        P("ra"),
        P("ra", "cb"),
        P("ra", "cb"),
        P("cb", "ra"),
    )
    return jax.shard_map(
        per_device, mesh=mesh, in_specs=placed, out_specs=P(None, "ra"), check_vma=False
    )
```

profile of v0, /device:TPU:0, one launch (start us, length us, event | category | flops | bytes accessed | tf_op | source)
XLA Modules:
  0.0 224.6 jit_solution(7267552355934892765)
XLA Ops:
  6.5 0.0 all-reduce.7.cloned.1.call-start
  6.5 0.9 fusion.14
  7.4 23.1 %psum.56 = f32[64]{0:T(128)S(1)} all-reduce(f32[64]{0:T(128)S(1)} %fusion.14), channel_id=1, replica_groups=mesh['ra'=8,'cb'=4] {'ra'}, use_global_device_ids=true, to_apply=%region_1.0 | all-reduce | flops 64 | bytes 512 | tf_op jit(solution)/shard_map/psum | solution.py:25
  30.6 0.0 copy-done.3
  30.6 0.0 copy-start.4
  30.6 1.9 fusion.8
  32.5 0.0 copy-done
  32.5 0.0 copy-done.4
  32.5 0.9 fusion.10
  33.4 0.0 all-reduce.7.cloned.1.call-update
  33.5 0.0 all-reduce.5.cloned.1.call-start
  33.5 69.4 %all-reduce.7.cloned.1.call-done = (f32[64,704]{1,0:T(8,128)}, f32[64,704]{1,0:T(8,128)}) async-done(((f32[64,704]{1,0:T(8,128)}, f32[64,704]{1,0:T(8,128)}), (f32[64,704]{1,0:T(8,128)}, f32[64,704]{1,0:T(8,128)})) %all-reduce.7.cloned.1.call-update) | async-done | bytes 360464 | tf_op jit(solution)/shard_map/psum | solution.py:13
  102.9 1.3 fusion.6
  104.1 0.0 copy-start.2
  104.2 10.4 %psum.59 = f32[64,128]{1,0:T(8,128)S(1)} all-reduce(f32[64,128]{1,0:T(8,128)S(1)} %fusion.6), channel_id=1, replica_groups=mesh['ra'=8,'cb'=4] {'cb'}, use_global_device_ids=true, to_apply=%region_4.5 | all-reduce | flops 8192 | bytes 65536 | tf_op jit(solution)/shard_map/psum | solution.py:31
  114.6 0.1 fusion.19
  114.7 19.5 %psum.60 = f32[64]{0:T(128)S(1)} all-reduce(f32[64]{0:T(128)S(1)} %get-tuple-element.9), channel_id=1, replica_groups=mesh['ra'=8,'cb'=4] {'ra'}, use_global_device_ids=true, to_apply=%region_6.7 | all-reduce | flops 64 | bytes 512 | tf_op jit(solution)/shard_map/psum | solution.py:25
  134.2 0.9 fusion.2
  135.1 0.9 fusion.4
  136.1 0.0 all-reduce.5.cloned.1.call-update
  136.1 69.6 %all-reduce.5.cloned.1.call-done = (f32[64,704]{1,0:T(8,128)}, f32[64,704]{1,0:T(8,128)}) async-done(((f32[64,704]{1,0:T(8,128)}, f32[64,704]{1,0:T(8,128)}), (f32[64,704]{1,0:T(8,128)}, f32[64,704]{1,0:T(8,128)})) %all-reduce.5.cloned.1.call-update) | async-done | bytes 360464 | tf_op jit(solution)/shard_map/psum | solution.py:13
  205.7 1.2 fusion
  206.9 10.3 %psum.63 = f32[64,128]{1,0:T(8,128)S(1)} all-reduce(f32[64,128]{1,0:T(8,128)S(1)} %fusion), channel_id=1, replica_groups=mesh['ra'=8,'cb'=4] {'cb'}, use_global_device_ids=true, to_apply=%region_9.10 | all-reduce | flops 8192 | bytes 65536 | tf_op jit(solution)/shard_map/psum | solution.py:31
  217.2 0.6 fusion.18
  (13 shorter events, 0.0 us)
Async XLA Ops:
  6.5 24.0 %copy-start.3 = (bf16[64,128]{1,0:T(8,128)(2,1)S(1)}, bf16[64,128]{1,0:T(8,128)(2,1)}, u32[]{:S(2)}) copy-start(bf16[64,128]{1,0:T(8,128)(2,1)} %param.9) | copy-start | bytes 49156
  6.5 26.0 %copy-start = (f32[128,704]{0,1:T(8,128)S(1)}, f32[128,704]{0,1:T(8,128)}, u32[]{:S(2)}) copy-start(f32[128,704]{0,1:T(8,128)} %param.11) | copy-start | bytes 1081348
  6.5 96.3 %all-reduce.7.cloned.1.call-start = ((), (), s32[]{:S(2)}) async-start(), calls=%async_computation.1 | async-start | bytes 786432 | tf_op jit(solution)/shard_map/psum | solution.py:13
  30.6 1.9 copy-start.4
  32.5 70.4 %copy-start.6 = (f32[704,128]{1,0:T(8,128)S(1)}, f32[704,128]{1,0:T(8,128)}, u32[]{:S(2)}) copy-start(f32[704,128]{1,0:T(8,128)} %param.13) | copy-start | bytes 1081348
  33.5 172.2 %all-reduce.5.cloned.1.call-start = ((), (), s32[]{:S(2)}) async-start(), calls=%async_computation | async-start | bytes 786432 | tf_op jit(solution)/shard_map/psum | solution.py:13
  102.9 31.3 %copy-start.1 = (f32[128,704]{0,1:T(8,128)S(1)}, f32[128,704]{0,1:T(8,128)}, u32[]{:S(2)}) copy-start(f32[128,704]{0,1:T(8,128)} %param.16) | copy-start | bytes 1081348
  102.9 31.3 %copy-start.5 = (f32[128]{0:T(128)S(1)}, f32[128]{0:T(128)}, u32[]{:S(2)}) copy-start(f32[128]{0:T(128)} %param.14) | copy-start | bytes 1540
  104.1 31.0 %copy-start.2 = (f32[128,704]{0,1:T(8,128)S(1)}, f32[128,704]{0,1:T(8,128)}, u32[]{:S(2)}) copy-start(f32[128,704]{0,1:T(8,128)} %param.15) | copy-start | bytes 1081348
  135.1 70.5 %copy-start.7 = (f32[704,128]{1,0:T(8,128)S(1)}, f32[704,128]{1,0:T(8,128)}, u32[]{:S(2)}) copy-start(f32[704,128]{1,0:T(8,128)} %param.17) | copy-start | bytes 1081348
Sparse Core Ops, SparseCore 0:
  33.6 69.2 all-reduce.6
  136.2 69.4 all-reduce.4
where the time goes:
time: 225 us
  waiting for transfers between devices  139 us (62%)
  blocking collectives  63.3 us (28%)
  between operations  13.5 us (6%)
  matrix products  7.15 us (3%)
    psum x2, waiting for transfers between devices, hidden_of(): gate_sum, up_sum = lax.psum((gate_part, up_part), 'ra')  139 us
    psum x2, blocking collectives, whole_sublayer(): square_total = lax.psum(jnp.sum(as_float * as_float, axis=1), 'ra')  42.7 us
    psum x2, blocking collectives, whole_sublayer(): branch = lax.psum(branch_part, 'cb')  20.7 us
  transfers between devices with their start and end apart: 2, of which 2 were waited for; matrix products, arithmetic and copies ran while one was open for 0% of the time, Pallas kernels for 0%

commit v1 on v0

--- a/solution.py
+++ b/solution.py
@@ -5,6 +5,12 @@
 
 residual_weight = 0.5
 epsilon = 1e-06
+
+
+def summed_here(x, name):
+    shards = lax.all_gather(x, name, axis=0, tiled=False)
+    summed = shards.sum(axis=0)
+    return summed
 
 
 def hidden_of(normed, gate_cast, up_cast):
@@ -28,7 +34,7 @@
     branch_part = jnp.dot(
         hidden, down_weight.astype(jnp.bfloat16), preferred_element_type=jnp.float32
     )
-    branch = lax.psum(branch_part, "cb")
+    branch = summed_here(branch_part, "cb")
     return (residual_weight * as_float + branch).astype(jnp.bfloat16)
 
 

time: 225 us -> 215 us (0.956)
  blocking collectives: 63.3 us -> 53.6 us
    psum x2 -> x0, blocking collectives: 20.7 us -> none  [whole_sublayer(): branch = lax.psum(branch_part, 'cb')]
    all_gather x0 -> x2, blocking collectives: none -> 11 us  [summed_here(): shards = lax.all_gather(x, name, axis=0, tiled=False)]
where the time goes in v1:
time: 215 us
  waiting for transfers between devices  139 us (65%)
  blocking collectives  53.6 us (25%)
  between operations  13.5 us (6%)
  matrix products  7.1 us (3%)
    psum x2, waiting for transfers between devices, hidden_of(): gate_sum, up_sum = lax.psum((gate_part, up_part), 'ra')  139 us
    psum x2, blocking collectives, whole_sublayer(): square_total = lax.psum(jnp.sum(as_float * as_float, axis=1), 'ra')  42.7 us
    all_gather x2, blocking collectives, summed_here(): shards = lax.all_gather(x, name, axis=0, tiled=False)  11 us
  transfers between devices with their start and end apart: 2, of which 2 were waited for; matrix products, arithmetic and copies ran while one was open for 0% of the time, Pallas kernels for 0%

profile of v1, /device:TPU:0, one launch (start us, length us, event | category | flops | bytes accessed | tf_op | source)
XLA Modules:
  0.0 214.7 jit_solution(11234577570022851380)
XLA Ops:
  6.5 0.0 all-reduce.7.cloned.1.call-start
  6.5 0.9 fusion.14
  7.4 23.1 %psum.42 = f32[64]{0:T(128)S(1)} all-reduce(f32[64]{0:T(128)S(1)} %fusion.14), channel_id=1, replica_groups=mesh['ra'=8,'cb'=4] {'ra'}, use_global_device_ids=true, to_apply=%region_1.0 | all-reduce | flops 64 | bytes 512 | tf_op jit(solution)/shard_map/psum | solution.py:31
  30.6 0.0 copy-start.4
  30.6 1.9 fusion.8
  32.5 0.0 copy-done
  32.5 0.9 fusion.10
  33.4 0.0 all-reduce.7.cloned.1.call-update
  33.5 0.0 all-reduce.5.cloned.1.call-start
  33.5 69.4 %all-reduce.7.cloned.1.call-done = (f32[64,704]{1,0:T(8,128)}, f32[64,704]{1,0:T(8,128)}) async-done(((f32[64,704]{1,0:T(8,128)}, f32[64,704]{1,0:T(8,128)}), (f32[64,704]{1,0:T(8,128)}, f32[64,704]{1,0:T(8,128)})) %all-reduce.7.cloned.1.call-update) | async-done | bytes 360464 | tf_op jit(solution)/shard_map/psum | solution.py:19
  102.9 1.2 fusion.6
  104.1 0.0 copy-start.1
  104.1 5.5 %all-gather = f32[256,128]{1,0:T(8,128)S(1)} all-gather(f32[64,128]{1,0:T(8,128)S(1)} %fusion.6), channel_id=2, replica_groups=mesh['ra'=8,'cb'=4] {'cb'}, dimensions={0}, use_global_device_ids=true | all-gather | bytes 163840 | tf_op jit(solution)/shard_map/all_gather | solution.py:11
  109.7 0.0 copy-start.2
  109.7 0.1 fusion.19
  109.8 19.5 %psum.45 = f32[64]{0:T(128)S(1)} all-reduce(f32[64]{0:T(128)S(1)} %get-tuple-element.9), channel_id=1, replica_groups=mesh['ra'=8,'cb'=4] {'ra'}, use_global_device_ids=true, to_apply=%region_6.7 | all-reduce | flops 64 | bytes 512 | tf_op jit(solution)/shard_map/psum | solution.py:31
  129.3 0.0 copy-done.1
  129.3 0.9 fusion.2
  130.3 0.9 fusion.4
  131.2 0.0 all-reduce.5.cloned.1.call-update
  131.2 69.3 %all-reduce.5.cloned.1.call-done = (f32[64,704]{1,0:T(8,128)}, f32[64,704]{1,0:T(8,128)}) async-done(((f32[64,704]{1,0:T(8,128)}, f32[64,704]{1,0:T(8,128)}), (f32[64,704]{1,0:T(8,128)}, f32[64,704]{1,0:T(8,128)})) %all-reduce.5.cloned.1.call-update) | async-done | bytes 360464 | tf_op jit(solution)/shard_map/psum | solution.py:19
  200.6 1.2 fusion
  201.8 5.4 %all-gather.1 = f32[256,128]{1,0:T(8,128)S(1)} all-gather(f32[64,128]{1,0:T(8,128)S(1)} %fusion), channel_id=3, replica_groups=mesh['ra'=8,'cb'=4] {'cb'}, dimensions={0}, use_global_device_ids=true | all-gather | bytes 163840 | tf_op jit(solution)/shard_map/all_gather | solution.py:11
  207.2 0.6 fusion.18
  (15 shorter events, 0.1 us)
Async XLA Ops:
  6.5 24.0 %copy-start.3 = (bf16[64,128]{1,0:T(8,128)(2,1)S(1)}, bf16[64,128]{1,0:T(8,128)(2,1)}, u32[]{:S(2)}) copy-start(bf16[64,128]{1,0:T(8,128)(2,1)} %param.9) | copy-start | bytes 49156
  6.5 26.0 %copy-start = (f32[128,704]{0,1:T(8,128)S(1)}, f32[128,704]{0,1:T(8,128)}, u32[]{:S(2)}) copy-start(f32[128,704]{0,1:T(8,128)} %param.11) | copy-start | bytes 1081348
  6.5 96.3 %all-reduce.7.cloned.1.call-start = ((), (), s32[]{:S(2)}) async-start(), calls=%async_computation.1 | async-start | bytes 786432 | tf_op jit(solution)/shard_map/psum | solution.py:19
  30.6 1.9 copy-start.4
  32.5 70.4 %copy-start.6 = (f32[704,128]{1,0:T(8,128)S(1)}, f32[704,128]{1,0:T(8,128)}, u32[]{:S(2)}) copy-start(f32[704,128]{1,0:T(8,128)} %param.13) | copy-start | bytes 1081348
  33.5 167.1 %all-reduce.5.cloned.1.call-start = ((), (), s32[]{:S(2)}) async-start(), calls=%async_computation | async-start | bytes 786432 | tf_op jit(solution)/shard_map/psum | solution.py:19
  104.1 25.2 %copy-start.1 = (f32[128,704]{0,1:T(8,128)S(1)}, f32[128,704]{0,1:T(8,128)}, u32[]{:S(2)}) copy-start(f32[128,704]{0,1:T(8,128)} %param.16) | copy-start | bytes 1081348
  109.7 19.7 %copy-start.5 = (f32[128]{0:T(128)S(1)}, f32[128]{0:T(128)}, u32[]{:S(2)}) copy-start(f32[128]{0:T(128)} %param.14) | copy-start | bytes 1540
  109.7 20.6 %copy-start.2 = (f32[128,704]{0,1:T(8,128)S(1)}, f32[128,704]{0,1:T(8,128)}, u32[]{:S(2)}) copy-start(f32[128,704]{0,1:T(8,128)} %param.15) | copy-start | bytes 1081348
  130.3 70.3 %copy-start.7 = (f32[704,128]{1,0:T(8,128)S(1)}, f32[704,128]{1,0:T(8,128)}, u32[]{:S(2)}) copy-start(f32[704,128]{1,0:T(8,128)} %param.17) | copy-start | bytes 1081348
Sparse Core Ops, SparseCore 0:
  33.6 69.2 all-reduce.6
  131.3 69.1 all-reduce.4
